TPU v7x, 128 devices: a whole 4x4x4 slice. The times are simulated.
128 devices in a mesh: fs: 32 (over z, y, core), tp: 4 (over x).
Axes of the slice: x: 4, y: 4, z: 4, core: 2. Of those that a mesh axis runs over, the one named last changes fastest.
Arguments:
- inputs: bfloat16 [65536, 2048], P('fs'), may hold values from -6 to 6
- attn_out: bfloat16 [65536, 1024], P('fs', 'tp'), may hold values from -6 to 6
- grad_query: bfloat16 [65536, 1024], P('fs', 'tp'), may hold values from -0.0625 to 0.0625
- grad_key: bfloat16 [65536, 1024], P('fs', 'tp'), may hold values from -0.0625 to 0.0625
- grad_mixed: bfloat16 [65536, 2048], P('fs'), may hold values from -0.109375 to 0.109375
- query_weight: float32 [2048, 1024], P('fs', 'tp'), may hold values from -0.75 to 0.75
- key_weight: float32 [2048, 1024], P('fs', 'tp'), may hold values from -0.75 to 0.75
- out_weight: float32 [1024, 2048], P('tp', 'fs'), may hold values from -0.75 to 0.75
- factors: bfloat16 [3, 2048, 256], P(None, 'fs'), may hold values from -0.125 to 0.125
- moment_first: float32 [3, 256, 1024], P(None, 'fs', 'tp'), may hold values from -6 to 6
- moment_second: float32 [3, 256, 1024], P(None, 'fs', 'tp'), may hold values from 0.05 to 2
Outputs:
- step_query: float32 [2048, 1024], P('fs', 'tp')
- step_key: float32 [2048, 1024], P('fs', 'tp')
- step_out: float32 [1024, 2048], P('tp', 'fs')
- copy_query: bfloat16 [2048, 1024], P(None, 'tp')
- copy_key: bfloat16 [2048, 1024], P(None, 'tp')
- copy_out: bfloat16 [1024, 2048], P('tp')
- first_new: float32 [3, 256, 1024], P(None, 'fs', 'tp')
- second_new: float32 [3, 256, 1024], P(None, 'fs', 'tp')
All inputs are finite; a program needn't handle non-finite values.
Results may differ from a plain program's by a relative error of at most 0.006.
Values may be sent and summed in bfloat16 or wider, within the bound.
A program may use at most 128 MiB of HBM per device.

v0:
```python
import jax
import jax.numpy as jnp
from jax import lax
from jax.sharding import Mesh
from jax.sharding import PartitionSpec as P

RANK = 256
HW = 1024
FS = ("fs_0", "fs_1", "fs_2")
FS_TP = ("fs_0", "fs_1", "fs_2", "tp")


first_decay = 0.8
second_decay = 0.9
epsilon = 1e-08
learn_rate = 0.02


def in_blocks(x, dim, devices):
    before, after = (x.shape[:dim], x.shape[dim + 1 :])
    return jnp.moveaxis(x.reshape(*before, devices, -1, *after), dim, 0)


def sum_at_owner(x, axis, dim):
    devices = lax.axis_size(axis)
    pieces = lax.all_to_all(in_blocks(x, dim, devices), axis, 0, 0, tiled=True)
    return jnp.sum(pieces, axis=0)


def over_axes(x, axes):
    for axis in axes:
        x = lax.psum(x, axis)
    return x


def from_everyone(x, axis):
    copies = jnp.broadcast_to(x, (lax.axis_size(axis), *x.shape))
    return lax.all_to_all(copies, axis, split_axis=0, concat_axis=0, tiled=True)


def joined_along(pieces, dim):
    lengths = list(pieces.shape[1:])
    lengths[dim] *= pieces.shape[0]
    return jnp.moveaxis(pieces, 0, dim).reshape(lengths)


def gathered_copies(x, axis, dim):
    pieces = from_everyone(x, axis)
    return joined_along(pieces, dim)


def rows_first(arrays, axis, dims):
    turned = [jnp.moveaxis(a, dim, 0) for a, dim in zip(arrays, dims)]
    widths = [t[0].size for t in turned]
    both = jnp.concatenate([t.reshape(-1, w) for t, w in zip(turned, widths)], axis=1)
    out = lax.all_gather(both, axis, axis=0, tiled=True)
    pieces = jnp.split(out, [sum(widths[:k]) for k in range(1, len(widths))], axis=1)
    return tuple(
        (
            jnp.moveaxis(b.reshape(-1, *t.shape[1:]), 0, dim)
            for b, t, dim in zip(pieces, turned, dims)
        )
    )


def over_tokens(left_side, right_side):
    return jnp.dot(left_side.T, right_side, preferred_element_type=jnp.float32)


def moments_update(projected, old_first, old_second):
    first_new = first_decay * old_first + (1.0 - first_decay) * projected
    second_new = second_decay * old_second + (1.0 - second_decay) * projected * projected
    adam_ratio = first_new / (jnp.sqrt(second_new) + epsilon)
    return (first_new, second_new, adam_ratio)


def per_device(
    inputs,
    attn_out,
    grad_query,
    grad_key,
    grad_mixed,
    query_weight,
    key_weight,
    out_weight,
    factors,
    moment_first,
    moment_second,
):
    pairs = ((inputs, grad_query), (inputs, grad_key), (grad_mixed, attn_out))
    partial_value = []
    whole_factors = lax.all_gather(factors, FS, axis=1, tiled=True)
    for matrix_number in range(3):
        left_side, right_side = pairs[matrix_number]
        mapped = jnp.dot(
            left_side, whole_factors[matrix_number], preferred_element_type=jnp.float32
        )
        upper_part = mapped.astype(jnp.bfloat16)
        lower_part = (mapped - upper_part.astype(jnp.float32)).astype(jnp.bfloat16)
        partial_value.append(
            over_tokens(upper_part, right_side) + over_tokens(lower_part, right_side)
        )
    partial_sums = jnp.stack(partial_value)
    reduced = sum_at_owner(partial_sums, FS, 1)
    first_new, second_new, adam_ratio = moments_update(reduced, moment_first, moment_second)
    square_total = over_axes(jnp.sum(adam_ratio * adam_ratio), FS_TP)
    directions = gathered_copies(adam_ratio.astype(jnp.bfloat16), FS, 1)
    step_scale = lax.rsqrt(square_total / (3 * RANK * HW) + 1.0)
    step_query = step_scale * jnp.dot(factors[0], directions[0], preferred_element_type=jnp.float32)
    step_key = step_scale * jnp.dot(factors[1], directions[1], preferred_element_type=jnp.float32)
    step_out = step_scale * jnp.dot(factors[2], directions[2], preferred_element_type=jnp.float32).T
    new_query = (query_weight - learn_rate * step_query).astype(jnp.bfloat16)
    new_key = (key_weight - learn_rate * step_key).astype(jnp.bfloat16)
    new_out = (out_weight - learn_rate * step_out).astype(jnp.bfloat16)
    copy_query, copy_key, copy_out = rows_first((new_query, new_key, new_out), FS, (0, 0, 1))
    return (step_query, step_key, step_out, copy_query, copy_key, copy_out, first_new, second_new)


def solution(mesh):
    split = Mesh(mesh.devices.reshape(4, 4, 2, mesh.shape["tp"]), ("fs_0", "fs_1", "fs_2", "tp"))
    placed = (
        P(FS, None),
        P(FS, "tp"),
        P(FS, "tp"),
        P(FS, "tp"),
        P(FS, None),
        P(FS, "tp"),
        P(FS, "tp"),
        P("tp", FS),
        P(None, FS, None),
        P(None, FS, "tp"),
        P(None, FS, "tp"),
    )
    return jax.shard_map(
        per_device,
        mesh=split,
        in_specs=placed,
        out_specs=(
            P(FS, "tp"),
            P(FS, "tp"),
            P("tp", FS),
            P(None, "tp"),
            P(None, "tp"),
            P("tp", None),
            P(None, FS, "tp"),
            P(None, FS, "tp"),
        ),
        check_vma=False,
    )
```

profile of v0, /device:TPU:1, one launch (start us, length us, event | category | flops | bytes accessed | tf_op | source)
XLA Modules:
  0.0 191.2 jit_solution(15449256281408140338)
XLA Ops:
  7.2 0.0 copy-start
  7.2 0.0 all-gather.3.cloned.1.call-start
  7.2 0.7 all-gather.3.cloned.1.call-update
  7.9 51.0 %all-gather.3.cloned.1.call-done = bf16[3,2048,256]{2,1,0:T(8,128)(2,1)} async-done(((bf16[3,64,256]{2,1,0:T(8,128)(2,1)}), bf16[3,2048,256]{2,1,0:T(8,128)(2,1)}) %all-gather.3.cloned.1.call-update) | async-done | bytes 3145744 | tf_op jit(solution)/shard_map/all_gather | solution.py:92
  58.9 0.0 copy-start.12
  58.9 6.2 %fusion.5 = f32[2048,256]{1,0:T(8,128)S(1)} fusion(bf16[2048,2048]{1,0:T(8,128)(2,1)} %param.15, bf16[3,2048,256]{2,1,0:T(8,128)(2,1)} %all-gather.3.cloned.1.call-done), kind=kOutput, calls=%fused_computation.16 | convolution fusion | flops 2147483648 | bytes 11534336 | tf_op jit(solution)/shard_map/dot_general | solution.py:95
  65.2 0.0 copy-done
  65.2 0.5 fusion.9
  65.7 0.0 copy-start.13
  65.7 0.5 fusion
  66.2 0.0 copy-done.12
  66.2 1.4 copy-done.13
  67.6 0.0 copy-start.1
  67.6 2.5 %fusion.6 = f32[2048,256]{1,0:T(8,128)S(1)} fusion(bf16[2048,2048]{1,0:T(8,128)(2,1)S(1)} %copy-done.12, bf16[3,2048,256]{2,1,0:T(8,128)(2,1)S(1)} %copy-done.13), kind=kOutput, calls=%fused_computation.18 | convolution fusion | flops 2147483648 | bytes 11534336 | tf_op jit(solution)/shard_map/dot_general | solution.py:95
  70.0 0.0 copy-done.1
  70.0 0.5 fusion.12
  70.5 0.5 fusion.1
  71.0 0.0 copy-start.2
  71.0 2.5 %fusion.7 = f32[2048,256]{1,0:T(8,128)S(1)} fusion(bf16[2048,2048]{1,0:T(8,128)(2,1)S(1)} %copy-done.12, bf16[3,2048,256]{2,1,0:T(8,128)(2,1)S(1)} %copy-done.13), kind=kOutput, calls=%fused_computation.20 | convolution fusion | flops 2147483648 | bytes 11534336 | tf_op jit(solution)/shard_map/dot_general | solution.py:95
  73.5 0.0 copy-done.2
  73.5 0.5 fusion.15
  74.0 0.5 fusion.2
  74.4 0.0 copy-start.10
  74.5 0.0 copy-start.11
  74.5 0.1 maximum_bitcast_fusion
  74.5 0.0 copy-start.3
  74.5 0.0 copy-start.7
  74.5 0.0 copy-start.8
  74.6 0.0 copy-start.9
  74.6 19.5 %all_to_all.10 = f32[32,3,8,256]{3,2,1,0:T(8,128)S(1)} all-to-all(f32[32,3,8,256]{3,2,1,0:T(8,128)S(1)} %maximum_bitcast_fusion), channel_id=1, replica_groups=mesh['fs_0'=4,'fs_1'=4,'fs_2'=2,'tp'=4] {'fs_0','fs_1','fs_2'}, dimensions={0} | all-to-all | bytes 1572864 | tf_op jit(solution)/shard_map/all_to_all | solution.py:26
  94.0 0.1 reduce_sum.18
  94.1 0.0 copy-done.10
  94.1 0.0 copy-done.11
  94.1 0.6 multiply_reduce_fusion
  94.7 0.0 copy-start.5
  94.7 0.0 copy-start.6
  94.8 0.8 broadcast_in_dim.3
  95.5 4.0 %all-to-all-start.1 = ((bf16[32,3,8,256]{3,2,1,0:T(8,128)(2,1)}), bf16[32,3,8,256]{3,2,1,0:T(8,128)(2,1)S(1)}, u32[]{:S(2)}, u32[]{:S(2)}) async-start(bf16[32,3,8,256]{3,2,1,0:T(8,128)(2,1)} %broadcast_in_dim.3), calls=%async_computation.1 | async-start | bytes 786432 | tf_op jit(solution)/shard_map/all_to_all | solution.py:38
  99.6 0.0 all-gather.5.cloned.1.call-start
  99.6 10.0 %psum.28 = f32[]{:T(128)} all-reduce(f32[]{:T(128)} %get-tuple-element.24), channel_id=1, replica_groups=mesh['fs_0'=4,'fs_1'=4,'fs_2'=2,'tp'=4] {'fs_0'}, use_global_device_ids=true, to_apply=%region_2.0 | all-reduce | flops 1 | bytes 8 | tf_op jit(solution)/shard_map/psum | solution.py:32
  109.6 8.7 %psum.29 = f32[]{:T(128)} all-reduce(f32[]{:T(128)} %psum.28), channel_id=1, replica_groups=mesh['fs_0'=4,'fs_1'=4,'fs_2'=2,'tp'=4] {'fs_1'}, use_global_device_ids=true, to_apply=%region_3.0 | all-reduce | flops 1 | bytes 8 | tf_op jit(solution)/shard_map/psum | solution.py:32
  118.4 6.9 %psum.30 = f32[]{:T(128)} all-reduce(f32[]{:T(128)} %psum.29), channel_id=1, replica_groups=mesh['fs_0'=4,'fs_1'=4,'fs_2'=2,'tp'=4] {'fs_2'}, use_global_device_ids=true, to_apply=%region_4.0 | all-reduce | flops 1 | bytes 8 | tf_op jit(solution)/shard_map/psum | solution.py:32
  125.3 9.0 %psum.31 = f32[]{:T(128)} all-reduce(f32[]{:T(128)} %psum.30), channel_id=1, replica_groups=mesh['fs_0'=4,'fs_1'=4,'fs_2'=2,'tp'=4] {'tp'}, use_global_device_ids=true, to_apply=%region_5.0 | all-reduce | flops 1 | bytes 8 | tf_op jit(solution)/shard_map/psum | solution.py:32
  135.0 0.0 all-to-all-done.1
  135.0 0.0 copy-done.3
  135.0 0.1 convolution_multiply_fusion
  135.1 0.0 copy-done.7
  135.2 0.0 copy-start.4
  135.2 0.8 subtract_convert_fusion.8
  136.0 0.0 copy-done.8
  136.0 0.8 subtract_convert_fusion.7
  136.7 0.0 copy-done.9
  136.8 0.6 pad_maximum_fusion
  137.4 0.0 all-gather.5.cloned.1.call-update
  137.4 42.0 %all-gather.5.cloned.1.call-done = bf16[2048,768]{1,0:T(8,128)(2,1)} async-done(((bf16[64,768]{1,0:T(8,128)(2,1)}), bf16[2048,768]{1,0:T(8,128)(2,1)}) %all-gather.5.cloned.1.call-update) | async-done | bytes 3145744 | tf_op jit(solution)/shard_map/all_gather | solution.py:56
  179.5 3.4 %slice_bitcast_fusion = (bf16[256,2048]{0,1:T(8,128)(2,1)S(1)}, bf16[2048,256]{1,0:T(8,128)(2,1)}, bf16[2048,256]{1,0:T(8,128)(2,1)}) fusion(bf16[2048,768]{1,0:T(8,128)(2,1)} %all-gather.5.cloned.1.call-done), kind=kLoop, calls=%fused_computation.14 | loop fusion | bytes 6291456 | tf_op jit(solution)/shard_map/transpose | solution.py:60
  182.9 0.0 copy-done.5
  182.9 0.0 copy-done.6
  182.9 0.0 copy-done.4
  182.9 1.4 copy.23
  (2 shorter events, 0.0 us)
Async XLA Ops:
  7.2 58.0 %copy-start = (bf16[2048,256]{1,0:T(8,128)(2,1)S(1)}, bf16[2048,256]{1,0:T(8,128)(2,1)}, u32[]{:S(2)}) copy-start(bf16[2048,256]{1,0:T(8,128)(2,1)} %param.12) | copy-start | bytes 3145732
  7.2 51.7 %all-gather.3.cloned.1.call-start = ((), (), s32[]{:S(2)}) async-start(), calls=%async_computation.2 | async-start | bytes 3244032 | tf_op jit(solution)/shard_map/all_gather | solution.py:92
  58.9 7.3 %copy-start.12 = (bf16[2048,2048]{1,0:T(8,128)(2,1)S(1)}, bf16[2048,2048]{1,0:T(8,128)(2,1)}, u32[]{:S(2)}) copy-start(bf16[2048,2048]{1,0:T(8,128)(2,1)} %param.11) | copy-start | bytes 25165828
  65.7 1.9 copy-start.13
  67.6 2.5 %copy-start.1 = (bf16[2048,256]{1,0:T(8,128)(2,1)S(1)}, bf16[2048,256]{1,0:T(8,128)(2,1)}, u32[]{:S(2)}) copy-start(bf16[2048,256]{1,0:T(8,128)(2,1)} %param.14) | copy-start | bytes 3145732
  71.0 2.5 %copy-start.2 = (bf16[2048,256]{1,0:T(8,128)(2,1)S(1)}, bf16[2048,256]{1,0:T(8,128)(2,1)}, u32[]{:S(2)}) copy-start(bf16[2048,256]{1,0:T(8,128)(2,1)} %param.13) | copy-start | bytes 3145732
  74.4 19.7 %copy-start.10 = (f32[3,8,256]{2,1,0:T(8,128)S(1)}, f32[3,8,256]{2,1,0:T(8,128)}, u32[]{:S(2)}) copy-start(f32[3,8,256]{2,1,0:T(8,128)} %param.21) | copy-start | bytes 73732
  74.5 19.7 %copy-start.11 = (f32[3,8,256]{2,1,0:T(8,128)S(1)}, f32[3,8,256]{2,1,0:T(8,128)}, u32[]{:S(2)}) copy-start(f32[3,8,256]{2,1,0:T(8,128)} %param.20) | copy-start | bytes 73732
  74.5 60.5 %copy-start.3 = (bf16[3,64,256]{2,1,0:T(8,128)(2,1)S(1)}, bf16[3,64,256]{2,1,0:T(8,128)(2,1)}, u32[]{:S(2)}) copy-start(bf16[3,64,256]{2,1,0:T(8,128)(2,1)} %param.19) | copy-start | bytes 294916
  74.5 60.6 %copy-start.7 = (f32[64,256]{1,0:T(8,128)S(1)}, f32[64,256]{1,0:T(8,128)}, u32[]{:S(2)}) copy-start(f32[64,256]{1,0:T(8,128)} %param.16) | copy-start | bytes 196612
  74.5 61.4 %copy-start.8 = (f32[64,256]{1,0:T(8,128)S(1)}, f32[64,256]{1,0:T(8,128)}, u32[]{:S(2)}) copy-start(f32[64,256]{1,0:T(8,128)} %param.17) | copy-start | bytes 196612
  74.6 62.2 %copy-start.9 = (f32[256,64]{0,1:T(8,128)S(1)}, f32[256,64]{0,1:T(8,128)}, u32[]{:S(2)}) copy-start(f32[256,64]{0,1:T(8,128)} %param.18) | copy-start | bytes 196612
  94.7 88.1 %copy-start.5 = (f32[3,8,256]{2,1,0:T(8,128)}, f32[3,8,256]{2,1,0:T(8,128)S(1)}, u32[]{:S(2)}) copy-start(f32[3,8,256]{2,1,0:T(8,128)S(1)} %get-tuple-element.25) | copy-start | bytes 73732
  94.7 88.1 %copy-start.6 = (f32[3,8,256]{2,1,0:T(8,128)}, f32[3,8,256]{2,1,0:T(8,128)S(1)}, u32[]{:S(2)}) copy-start(f32[3,8,256]{2,1,0:T(8,128)S(1)} %get-tuple-element.26) | copy-start | bytes 73732
  95.5 39.4 %all-to-all-start.1 = ((bf16[32,3,8,256]{3,2,1,0:T(8,128)(2,1)}), bf16[32,3,8,256]{3,2,1,0:T(8,128)(2,1)S(1)}, u32[]{:S(2)}, u32[]{:S(2)}) async-start(bf16[32,3,8,256]{3,2,1,0:T(8,128)(2,1)} %broadcast_in_dim.3), calls=%async_computation.1 | async-start | bytes 786432 | tf_op jit(solution)/shard_map/all_to_all | solution.py:38
  99.6 79.9 %all-gather.5.cloned.1.call-start = ((), (), s32[]{:S(2)}) async-start(), calls=%async_computation.3 | async-start | bytes 3244032 | tf_op jit(solution)/shard_map/all_gather | solution.py:56
  135.2 47.7 %copy-start.4 = (f32[256,64]{0,1:T(8,128)}, f32[256,64]{0,1:T(8,128)S(1)}, u32[]{:S(2)}) copy-start(f32[256,64]{0,1:T(8,128)S(1)} %convolution_multiply_fusion) | copy-start | bytes 196612
Sparse Core Ops, SparseCore 0:
  10.3 48.5 all-gather.2
  137.6 41.8 all-gather.4
where the time goes:
time: 192 us; the launch traced here: 191 us
  waiting for transfers between devices  93.7 us (49%)
  blocking collectives  54.1 us (28%)
  matrix products  15.7 us (8%)
  between operations  15 us (8%)
  local copies, waits for them, and re-layouts  7.06 us (4%)
  starting transfers between devices  4.13 us (2%)
    all_gather x1, waiting for transfers between devices, per_device(): whole_factors = lax.all_gather(factors, FS, axis=1, tiled=True)  51 us
    all_gather x1, waiting for transfers between devices, rows_first(): out = lax.all_gather(both, axis, axis=0, tiled=True)  42 us
    psum x4, blocking collectives, over_axes(): x = lax.psum(x, axis)  34.6 us
    all_to_all x1, blocking collectives, sum_at_owner(): pieces = lax.all_to_all(in_blocks(x, dim, devices), axis, 0, 0, tiled=True)  19.5 us
    dot_general x3, matrix products, per_device(): jnp.dot(left_side, whole_factors[matrix_number], preferred_element_type=j...  11.1 us
    all_to_all x1, starting transfers between devices, from_everyone(): return lax.all_to_all(copies, axis, split_axis=0, concat_axis=0, tiled=True)  4.05 us
  transfers between devices with their start and end apart: 3, of which 2 were waited for; matrix products, arithmetic and copies ran while one was open for 0% of the time, Pallas kernels for 0%

commit v1 on v0

v1 whole, which is shorter than its diff:
```python
import jax
import jax.numpy as jnp
from jax import lax
from jax.experimental import pallas as pl
from jax.experimental.pallas import tpu as pltpu
from jax.sharding import Mesh
from jax.sharding import PartitionSpec as P

RANK = 256
HW = 1024
FS = ("z", "y", "c")
MESH = pl.DeviceIdType.MESH
bf16 = jnp.bfloat16
f32 = jnp.float32

first_decay = 0.8
second_decay = 0.9
epsilon = 1e-08
learn_rate = 0.02

ROUNDS = (
    ((0, 1), (0, 3), (1, 0), (3, 0)),
    ((1, 1), (1, 3), (3, 1), (3, 3), (0, 2), (2, 0)),
    ((1, 2), (3, 2), (2, 1), (2, 3)),
    ((2, 2),),
)


def wrap(v):
    return lax.rem(v, 4)


class Gather:
    def __init__(self, buf, recv, send, pair_recv, pair_send, where):
        self.buf, self.recv, self.send = buf, recv, send
        self.pair_recv, self.pair_send, self.where = pair_recv, pair_send, where
        self.started = []
        self.count = [0, 0]

    def device(self, dz, dy, other=False):
        z, y, c, x = self.where
        return (wrap(z + dz), wrap(y + dy), 1 - c if other else c, x)

    def block(self, a, b, half, quarter):
        z, y, c, x = self.where
        dz, dy = (b, a) if half == 0 else (a, b)
        zs, ys = wrap(z + 4 - dz), wrap(y + 4 - dy)
        start, size = (32 * half, 32) if quarter is None else (32 * half + 16 * quarter, 16)
        return self.buf.at[:, zs, ys, c, pl.ds(start, size)], (half, zs, ys, quarter or 0)

    def copy(self, a, b, half, quarter, to, other=False):
        ref, index = self.block(a, b, half, quarter)
        recv = self.pair_recv if other else self.recv
        sems = self.pair_send if other else self.send
        n = self.count[other]
        self.count[other] += 1
        cp = pltpu.make_async_remote_copy(
            src_ref=ref,
            dst_ref=ref,
            send_sem=sems.at[n],
            recv_sem=recv.at[index[:3]] if other else recv.at[index],
            device_id=to,
            device_id_type=MESH,
        )
        cp.start()
        self.started.append(cp)

    def steps(self, half, dim, amount):
        moves_y = (dim == 0) == (half == 0)
        return self.device(0, amount) if moves_y else self.device(amount, 0)

    def wait(self, a, b, half, quarter):
        ref, index = self.block(a, b, half, quarter)
        pltpu.make_async_remote_copy(
            src_ref=ref,
            dst_ref=ref,
            send_sem=self.send.at[0],
            recv_sem=self.recv.at[index],
            device_id=self.where,
            device_id_type=MESH,
        ).wait_recv()

    def own(self):
        for half in range(2):
            for dim in range(2):
                self.copy(0, 0, half, None, self.steps(half, dim, 1))
                self.copy(0, 0, half, None, self.steps(half, dim, 3))
        for half in range(2):
            self.copy(0, 0, half, None, self.device(0, 0, True), True)

    def round(self, number):
        for a, b in ROUNDS[number]:
            for half in range(2):
                if b == 2 or (b == 0 and a == 2):
                    self.wait(a, b, half, 0)
                    self.wait(a, b, half, 1)
                else:
                    self.wait(a, b, half, None)
                if b == 0:
                    if a == 1:
                        self.copy(a, b, half, 0, self.steps(half, 0, 1))
                    if a == 3:
                        self.copy(a, b, half, 1, self.steps(half, 0, 3))
                    self.copy(a, b, half, None, self.steps(half, 1, 1))
                    self.copy(a, b, half, None, self.steps(half, 1, 3))
                elif b == 1:
                    self.copy(a, b, half, 0, self.steps(half, 1, 1))
                elif b == 3:
                    self.copy(a, b, half, 1, self.steps(half, 1, 3))
                self.copy(a, b, half, None, self.device(0, 0, True), True)

    def from_pair(self):
        z, y, c, x = self.where
        for half in range(2):
            for zs in range(4):
                for ys in range(4):
                    ref = self.buf.at[:, zs, ys, 1 - c, pl.ds(32 * half, 32)]
                    pltpu.make_async_remote_copy(
                        src_ref=ref,
                        dst_ref=ref,
                        send_sem=self.send.at[0],
                        recv_sem=self.pair_recv.at[half, zs, ys],
                        device_id=self.where,
                        device_id_type=MESH,
                    ).wait_recv()

    def finish(self):
        for cp in self.started:
            cp.wait_send()


def exchange_kernel(
    inputs, attn_out, grad_query, grad_key, grad_mixed, query_weight, key_weight, out_weight, factors, moment_first, moment_second,
    fg, wg, rg, first_new, second_new, squares,
    left, right, right_t, grad_t, weights, old_first, old_second, partial, from_core, chip_sum, arrived, sq_arrived,
    f_recv, f_send, f_pair_recv, f_pair_send,
    w_recv, w_send, w_pair_recv, w_pair_send,
    p_pair, p_recv, p_send, r_recv, r_send, r_pair, sq_recv, sq_send,
    local, left_sem, right_sem,
):
    z, y, c, x = where = tuple(lax.axis_index(a) for a in ("z", "y", "c", "x"))
    chip = z * 4 + y
    partner = (z, y, 1 - c, x)

    barrier = pltpu.get_barrier_semaphore()
    greeted = [
        (wrap(z + 1), y, c, x), (wrap(z + 3), y, c, x), (z, wrap(y + 1), c, x), (z, wrap(y + 3), c, x), partner,
        (z, y, c, wrap(x + 1)), (z, y, c, wrap(x + 2)), (z, y, c, wrap(x + 3)),
    ]
    for other in greeted:
        pl.semaphore_signal(barrier, inc=1, device_id=other, device_id_type=MESH)

    own_factors = pltpu.make_async_copy(factors, fg.at[:, z, y, c], local.at[0])
    own_factors.start()
    right_loads = []
    for m, ref in enumerate((grad_query, grad_key, attn_out)):
        right_loads.append(pltpu.make_async_copy(ref, right.at[m], right_sem.at[m]))
    left_loads = []
    for m, ref in enumerate((inputs, grad_mixed)):
        for n in range(4):
            columns = pl.ds(512 * n, 512)
            left_loads.append(pltpu.make_async_copy(ref.at[:, columns], left.at[m, n], left_sem.at[m, n]))
    small = [
        pltpu.make_async_copy(query_weight, weights.at[0], local.at[1]),
        pltpu.make_async_copy(key_weight, weights.at[1], local.at[2]),
        pltpu.make_async_copy(out_weight, weights.at[2], local.at[3]),
        pltpu.make_async_copy(moment_first, old_first, local.at[4]),
        pltpu.make_async_copy(moment_second, old_second, local.at[5]),
    ]
    right_loads[0].start()
    right_loads[1].start()
    for cp in small:
        cp.start()
    left_loads[0].start()
    left_loads[1].start()
    right_loads[2].start()
    for cp in left_loads[2:]:
        cp.start()

    pl.semaphore_wait(barrier, len(greeted))
    own_factors.wait()
    gf = Gather(fg, f_recv, f_send, f_pair_recv, f_pair_send, where)
    gw = Gather(wg, w_recv, w_send, w_pair_recv, w_pair_send, where)
    gf.own()

    for cp in small:
        cp.wait()
    wg[0, z, y, c] = weights[0].astype(bf16)
    wg[1, z, y, c] = weights[1].astype(bf16)
    wg[2, z, y, c] = weights[2].astype(bf16)

    def turn(m):
        right_loads[m].wait()
        for n in range(4):
            rows = pl.ds(512 * n, 512)
            right_t[pl.ds(256 * m, 256), rows] = right[m, rows, :].T

    def query_key(n):
        left_loads[n].wait()
        for h in range(2):
            product = jnp.dot(right_t[0:512, :], left[0, n, :, 256 * h : 256 * h + 256], preferred_element_type=f32)
            grad_t[0:512, 512 * n + 256 * h : 512 * n + 256 * h + 256] = product.astype(bf16)

    def output(n):
        left_loads[4 + n].wait()
        product = jnp.dot(right_t[512:768, :], left[1, n], preferred_element_type=f32)
        grad_t[512:768, 512 * n : 512 * n + 512] = product.astype(bf16)

    turn(0)
    turn(1)
    query_key(0)
    gf.round(0)
    query_key(1)
    query_key(2)
    gf.round(1)
    gw.own()
    query_key(3)
    turn(2)
    output(0)
    gf.round(2)
    output(1)
    output(2)
    gf.round(3)
    gw.round(0)
    output(3)
    gf.from_pair()

    for m in range(3):
        projected = jnp.dot(grad_t[256 * m : 256 * m + 256, :], fg[m].reshape(2048, RANK), preferred_element_type=f32)
        projected = projected.T.reshape(32, 8, 256)
        packed = jnp.concatenate([projected[:, :, :128], projected[:, :, 128:]], axis=1).astype(bf16)
        partial[:, :, :, 128 * m : 128 * m + 128] = packed.reshape(16, 2, 16, 128)

    pair_copy = pltpu.make_async_remote_copy(
        src_ref=partial.at[:, 1 - c], dst_ref=from_core, send_sem=p_pair.at[0], recv_sem=p_pair.at[1],
        device_id=partner, device_id_type=MESH,
    )
    pair_copy.start()
    gw.round(1)
    pair_copy.wait_recv()
    chip_sum[...] = (partial[:, c].astype(f32) + from_core[...].astype(f32)).astype(bf16)

    offsets = [(dz, dy) for dz in range(4) for dy in range(4) if (dz, dy) != (0, 0)]
    offsets.sort(key=lambda o: -(min(o[0], 4 - o[0]) + min(o[1], 4 - o[1])))
    p_copies = []
    for k, (dz, dy) in enumerate(offsets):
        tz, ty = wrap(z + dz), wrap(y + dy)
        cp = pltpu.make_async_remote_copy(
            src_ref=chip_sum.at[tz * 4 + ty], dst_ref=arrived.at[k], send_sem=p_send.at[k], recv_sem=p_recv.at[k],
            device_id=(tz, ty, c, x), device_id_type=MESH,
        )
        cp.start()
        p_copies.append(cp)
    gw.round(2)
    total = chip_sum[chip].astype(f32)
    for k in reversed(range(15)):
        p_copies[k].wait_recv()
        total = total + arrived[k].astype(f32)

    ratios = []
    for m in range(3):
        lanes = slice(128 * m, 128 * m + 128)
        p = jnp.concatenate([total[0:8, lanes], total[8:16, lanes]], axis=1)
        first = first_decay * old_first[m] + (1.0 - first_decay) * p
        second = second_decay * old_second[m] + (1.0 - second_decay) * p * p
        first_new[m] = first
        second_new[m] = second
        ratio = first / (jnp.sqrt(second) + epsilon)
        ratios.append(jnp.concatenate([ratio[:, :128], ratio[:, 128:]], axis=0))
    rg[chip, c] = jnp.concatenate(ratios, axis=1).astype(bf16)

    r_copies = []
    for k, (dz, dy) in enumerate(offsets):
        tz, ty = wrap(z + dz), wrap(y + dy)
        r_copies.append(
            pltpu.make_async_remote_copy(
                src_ref=rg.at[chip, c], dst_ref=rg.at[chip, c], send_sem=r_send.at[k], recv_sem=r_recv.at[k],
                device_id=(tz, ty, c, x), device_id_type=MESH,
            )
        )
        r_copies[-1].start()
    gw.round(3)
    for k, (dz, dy) in enumerate(offsets):
        source = wrap(z + 4 - dz) * 4 + wrap(y + 4 - dy)
        pltpu.make_async_remote_copy(
            src_ref=rg.at[source, c], dst_ref=rg.at[source, c], send_sem=r_send.at[k], recv_sem=r_recv.at[k],
            device_id=where, device_id_type=MESH,
        ).wait_recv()
    r_forward = pltpu.make_async_remote_copy(
        src_ref=rg.at[:, c], dst_ref=rg.at[:, c], send_sem=r_pair.at[0], recv_sem=r_pair.at[1],
        device_id=partner, device_id_type=MESH,
    )
    r_forward.start()
    gw.from_pair()
    pltpu.make_async_remote_copy(
        src_ref=rg.at[:, 1 - c], dst_ref=rg.at[:, 1 - c], send_sem=r_pair.at[0], recv_sem=r_pair.at[1],
        device_id=partner, device_id_type=MESH,
    ).wait_recv()

    everyone = rg[...].astype(f32)
    squared = jnp.sum((everyone * everyone).reshape(64, 8, 384), axis=0)
    sq_arrived[0] = squared[:, :128] + squared[:, 128:256] + squared[:, 256:]
    s_copies = []
    for k in range(1, 4):
        s_copies.append(
            pltpu.make_async_remote_copy(
                src_ref=sq_arrived.at[0], dst_ref=sq_arrived.at[k], send_sem=sq_send.at[k - 1], recv_sem=sq_recv.at[k - 1],
                device_id=(z, y, c, wrap(x + k)), device_id_type=MESH,
            )
        )
        s_copies[-1].start()
    for cp in s_copies:
        cp.wait_recv()
    squares[...] = sq_arrived[0] + sq_arrived[1] + sq_arrived[2] + sq_arrived[3]

    gf.finish()
    gw.finish()
    pair_copy.wait_send()
    r_forward.wait_send()
    for cp in p_copies + r_copies + s_copies:
        cp.wait_send()


def step_kernel(
    fg, wg, rg, first_in, second_in, squares, factors,
    step_query, step_key, step_out, copy_query, copy_key, copy_out, first_new, second_new, ratios,
):
    i = pl.program_id(0)
    scale = lax.rsqrt(jnp.sum(squares[...], keepdims=True) / (3 * RANK * HW) + 1.0)

    @pl.when(i == 0)
    def _():
        first_new[...] = first_in[...]
        second_new[...] = second_in[...]
        for m in range(3):
            part = rg[:, :, :, 128 * m : 128 * m + 128].astype(f32).reshape(32, 16, 128)
            whole = jnp.concatenate([part[:, :8], part[:, 8:]], axis=2).reshape(RANK, 256)
            ratios[m] = whole.astype(bf16)
        ratios[3] = whole.T.astype(bf16)
        for m, out in enumerate((step_query, step_key, step_out)):
            out[...] = scale * jnp.dot(factors[m], ratios[m], preferred_element_type=f32)

    rate = learn_rate * scale
    for m, out in ((0, copy_query), (1, copy_key)):
        change = jnp.dot(fg[m, i].reshape(512, RANK), ratios[m], preferred_element_type=f32)
        out[...] = (wg[m, i].reshape(512, 256).astype(f32) - rate * change).astype(bf16)
    change = lax.dot_general(ratios[3], fg[2, i].reshape(512, RANK), (((1,), (1,)), ((), ())), preferred_element_type=f32)
    copy_out[...] = (wg[2, i].reshape(512, 256).astype(f32).T - rate * change).astype(bf16)


def per_device(*args):
    sem = pltpu.SemaphoreType.DMA
    vmem = pl.BlockSpec(memory_space=pltpu.VMEM)
    args = list(args)
    args[7] = args[7].T
    held = [pltpu.with_memory_space_constraint(a, pltpu.HBM) for a in args]
    outs = pl.pallas_call(
        exchange_kernel,
        out_shape=(
            pltpu.VMEM((3, 4, 4, 2, 64, 256), bf16),
            pltpu.VMEM((3, 4, 4, 2, 64, 256), bf16),
            pltpu.VMEM((16, 2, 16, 384), bf16),
            pltpu.VMEM((3, 8, 256), f32),
            pltpu.VMEM((3, 8, 256), f32),
            pltpu.VMEM((8, 128), f32),
        ),
        in_specs=[pl.BlockSpec(memory_space=pltpu.HBM)] * 11,
        out_specs=(vmem,) * 6,
        scratch_shapes=[
            pltpu.VMEM((2, 4, 2048, 512), bf16),
            pltpu.VMEM((3, 2048, 256), bf16),
            pltpu.VMEM((768, 2048), bf16),
            pltpu.VMEM((768, 2048), bf16),
            pltpu.VMEM((3, 64, 256), f32),
            pltpu.VMEM((3, 8, 256), f32),
            pltpu.VMEM((3, 8, 256), f32),
            pltpu.VMEM((16, 2, 16, 384), bf16),
            pltpu.VMEM((16, 16, 384), bf16),
            pltpu.VMEM((16, 16, 384), bf16),
            pltpu.VMEM((15, 16, 384), bf16),
            pltpu.VMEM((4, 8, 128), f32),
            sem((2, 4, 4, 2)), sem((40,)), sem((2, 4, 4)), sem((32,)),
            sem((2, 4, 4, 2)), sem((40,)), sem((2, 4, 4)), sem((32,)),
            sem((2,)), sem((15,)), sem((15,)), sem((15,)), sem((15,)), sem((2,)), sem((3,)), sem((3,)),
            sem((6,)), sem((2, 4)), sem((3,)),
        ],
        compiler_params=pltpu.CompilerParams(collective_id=0, has_side_effects=True, vmem_limit_bytes=44 << 20),
        name="exchange",
    )(*held)
    fg, wg, rg, first_new, second_new, squares = [pltpu.with_memory_space_constraint(o, pltpu.VMEM) for o in outs]
    whole = lambda *shape: pl.BlockSpec(shape, lambda i: (0,) * len(shape))
    outs = pl.pallas_call(
        step_kernel,
        grid=(4,),
        in_specs=[vmem] * 7,
        out_specs=(
            whole(64, 256),
            whole(64, 256),
            whole(64, 256),
            pl.BlockSpec((512, 256), lambda i: (i, 0)),
            pl.BlockSpec((512, 256), lambda i: (i, 0)),
            pl.BlockSpec((256, 512), lambda i: (0, i)),
            whole(3, 8, 256),
            whole(3, 8, 256),
        ),
        out_shape=(
            jax.ShapeDtypeStruct((64, 256), f32),
            jax.ShapeDtypeStruct((64, 256), f32),
            jax.ShapeDtypeStruct((64, 256), f32),
            jax.ShapeDtypeStruct((2048, 256), bf16),
            jax.ShapeDtypeStruct((2048, 256), bf16),
            jax.ShapeDtypeStruct((256, 2048), bf16),
            jax.ShapeDtypeStruct((3, 8, 256), f32),
            jax.ShapeDtypeStruct((3, 8, 256), f32),
        ),
        scratch_shapes=[pltpu.VMEM((4, 256, 256), bf16)],
        compiler_params=pltpu.CompilerParams(vmem_limit_bytes=32 << 20),
        name="steps",
    )(fg, wg, rg, first_new, second_new, squares, args[8])
    return (*outs[:2], outs[2].T, *outs[3:])


def solution(mesh):
    split = Mesh(mesh.devices.reshape(4, 4, 2, mesh.shape["tp"]), ("z", "y", "c", "x"))
    placed = (
        P(FS, None),
        P(FS, "x"),
        P(FS, "x"),
        P(FS, "x"),
        P(FS, None),
        P(FS, "x"),
        P(FS, "x"),
        P("x", FS),
        P(None, FS, None),
        P(None, FS, "x"),
        P(None, FS, "x"),
    )
    return jax.shard_map(
        per_device,
        mesh=split,
        in_specs=placed,
        out_specs=(
            P(FS, "x"),
            P(FS, "x"),
            P("x", FS),
            P(None, "x"),
            P(None, "x"),
            P("x", None),
            P(None, FS, "x"),
            P(None, FS, "x"),
        ),
        check_vma=False,
    )
```

time: 192 us -> 56.8 us (0.30)
  waiting for transfers between devices: 93.7 us -> 0 us
  Pallas kernels: 0 us -> 56 us
  blocking collectives: 54.1 us -> 0 us
  matrix products: 15.7 us -> 0 us
  between operations: 15 us -> 0.66 us
  local copies, waits for them, and re-layouts: 7.06 us -> 0.01 us
  starting transfers between devices: 4.13 us -> 0 us
    all_gather x2 -> x0, waiting for transfers between devices: 93 us -> none  [the longest x1 51 us: per_device(): whole_factors = lax.all_gather(factors, FS, axis=1, tiled=True)]
    pallas_call x0 -> x2, Pallas kernels: none -> 56 us  [the longest x1 52.6 us: per_device(): pl.pallas_call(exchange_kernel, out_shape=(pltpu.VMEM((3, 4, 4, 2, 64, 25...]
    psum x4 -> x0, blocking collectives: 34.6 us -> none  [over_axes(): x = lax.psum(x, axis)]
    all_to_all x1 -> x0, blocking collectives: 19.5 us -> none  [sum_at_owner(): pieces = lax.all_to_all(in_blocks(x, dim, devices), axis, 0, 0, tiled=True)]
    dot_general x12 -> x0, matrix products: 15.7 us -> none  [the longest x3 11.1 us: per_device(): jnp.dot(left_side, whole_factors[matrix_number], preferred_element_type=j...]
    all_to_all x1 -> x0, starting transfers between devices: 4.05 us -> none  [from_everyone(): return lax.all_to_all(copies, axis, split_axis=0, concat_axis=0, tiled=True)]
    transpose x1 -> x0, local copies, waits for them, and re-layouts: 3.41 us -> none  [rows_first(): jnp.moveaxis(b.reshape(-1, *t.shape[1:]), 0, dim)]
    unnamed x29 -> x2, local copies, waits for them, and re-layouts: 2.88 us -> 0.01 us
  transfers between devices with their start and end apart: 3 -> 0, of which waited for: 2 -> 0; matrix products, arithmetic and copies ran while one was open for 0% -> 0% of each run, Pallas kernels for 0% -> 0%
where the time goes in v1:
time: 56.8 us; the launch traced here: 56.7 us
  Pallas kernels  56 us (99%)
  between operations  0.66 us (1%)
    pallas_call x1, Pallas kernels, per_device(): pl.pallas_call(exchange_kernel, out_shape=(pltpu.VMEM((3, 4, 4, 2, 64, 25...  52.6 us
    pallas_call x1, Pallas kernels, per_device(): pl.pallas_call(step_kernel, grid=(4,), in_specs=[vmem] * 7, out_specs=(wh...  3.46 us

profile of v1, /device:TPU:1, one launch (start us, length us, event | category | flops | bytes accessed | tf_op | source)
XLA Modules:
  0.0 56.7 jit_solution(5355019276149649206)
XLA Ops:
  0.6 0.0 copy-start
  0.6 52.6 %exchange.1 = (bf16[3,4,4,2,64,256]{5,4,3,2,1,0:T(8,128)(2,1)S(1)}, bf16[3,4,4,2,64,256]{5,4,3,2,1,0:T(8,128)(2,1)S(1)}, bf16[16,2,16,384]{3,2,1,0:T(8,128)(2,1)...) custom-call(bf16[2048,2048]{1,0:T(8,128)(2,1)} %inputs.1, ...), custom_call_target="tpu_custom_call" | custom-call | tf_op jit(solution)/shard_map/exchange/pallas_call | solution.py:357
  53.2 0.0 copy-done
  53.2 3.5 %steps.1 = (f32[64,256]{1,0:T(8,128)}, f32[64,256]{1,0:T(8,128)}, f32[64,256]{1,0:T(8,128)}, bf16[2048,256]{1,0:T(8,128)(2,1)}, bf16[2048,256]{1,0:T(8,128)(2,1)...) custom-call(bf16[3,4,4,2,64,256]{5,4,3,2,1,0:T(8,128)(2,1)S(1)} %get-tuple-element.22.fg, ...), custom_call_target="tpu_custom_call" | custom-call | tf_op jit(solution)/shard_map/steps/pallas_call | solution.py:392
Async XLA Ops:
  0.6 52.6 %copy-start = (bf16[3,64,256]{2,1,0:T(8,128)(2,1)S(1)}, bf16[3,64,256]{2,1,0:T(8,128)(2,1)}, u32[]{:S(2)}) copy-start(bf16[3,64,256]{2,1,0:T(8,128)(2,1)} %factors.3) | copy-start | bytes 294916
